TPU v7x, 32 devices: a whole 2x2x4 slice. The times are simulated.
32 devices in a mesh: ep: 16 (over z, y, x), tp: 2 (over core).
Axes of the slice: x: 2, y: 2, z: 4, core: 2. Of those that a mesh axis runs over, the one named last changes fastest.
Arguments:
- tokens: bfloat16 [512, 2048], P('ep'), may hold values from -6 to 6
- mix_gain: float32 [2048], replicated, may hold values from 0.1 to 1.9
- w_query: bfloat16 [2048, 512], P('ep', 'tp'), may hold values from -0.125 to 0.125
- w_key: bfloat16 [2048, 512], P('ep', 'tp'), may hold values from -0.125 to 0.125
- w_value: bfloat16 [2048, 512], P('ep', 'tp'), may hold values from -0.125 to 0.125
- w_outgate: bfloat16 [2048, 512], P('ep', 'tp'), may hold values from -0.125 to 0.125
- w_igate: bfloat16 [2048, 8], P('ep', 'tp'), may hold values from -0.125 to 0.125
- w_fgate: bfloat16 [2048, 8], P('ep', 'tp'), may hold values from -0.125 to 0.125
- igate_bias: float32 [8], P('tp'), may hold values from -2 to 1
- fgate_bias: float32 [8], P('tp'), may hold values from 0 to 4
- head_gain: float32 [512], P('tp'), may hold values from 0.1 to 1.9
- w_out: bfloat16 [512, 2048], P('tp', 'ep'), may hold values from -0.25 to 0.25
- state_matrix: float32 [512, 8, 64, 64], P('ep', 'tp'), may hold values from -2.4 to 2.4
- state_norm: float32 [512, 8, 64], P('ep', 'tp'), may hold values from -2.4 to 2.4
- state_max: float32 [512, 8], P('ep', 'tp'), may hold values from -4 to 4
- ffn_gain: float32 [2048], replicated, may hold values from 0.1 to 1.9
- w_expert_gate: bfloat16 [16, 2048, 1408], P('ep', None, 'tp'), may hold values from -0.125 to 0.125
- w_expert_up: bfloat16 [16, 2048, 1408], P('ep', None, 'tp'), may hold values from -0.125 to 0.125
- w_expert_down: bfloat16 [16, 1408, 2048], P('ep', 'tp'), may hold values from -0.15625 to 0.15625
- routes: int32 [512, 3], P('ep'), may hold values from 0 to 15, all different within a row; in each aligned block of 32 rows (0 to 31, 32 to 63, ...) at most 12 rows name the same one
- route_weights: float32 [512, 3], P('ep'), may hold values from 0.2 to 1
Outputs:
- mixed: bfloat16 [512, 2048], P('ep')
- new_matrix: float32 [512, 8, 64, 64], P('ep', 'tp')
- new_norm: float32 [512, 8, 64], P('ep', 'tp')
- new_max: float32 [512, 8], P('ep', 'tp')
Inputs may be any that keep to these rules, and one draw needn't show every extreme that they name: `routes`: each row names 3 different experts. Among the rows of one device, no expert is named by more than 12 rows, a bound that some block reaches.
All inputs are finite; a program needn't handle non-finite values.
Results may differ from a plain program's by a relative error of at most 0.017.
Values may be sent and summed in bfloat16 or wider, within the bound.
No kernel may reach another device: no remote copies, remote signals or barrier semaphores. Data moves between devices by JAX's collectives and lax.ppermute only.
A program may use at most 128 MiB of HBM per device.

v0:
```python
import jax
import jax.numpy as jnp
from jax import lax
from jax.sharding import PartitionSpec as P


def rms_scale(values_in, gain_vec):
    widened = values_in.astype(jnp.float32)
    return (
        widened * lax.rsqrt(jnp.mean(widened * widened, axis=-1, keepdims=True) + 1e-06) * gain_vec
    )


def memory_cell(
    query,
    key_row,
    value_row,
    outgate,
    input_pre,
    forget_pre,
    head_gain,
    state_matrix,
    state_norm,
    state_max,
):
    seq_rows, head_count = input_pre.shape
    head_size = query.shape[1] // head_count
    query_heads = query.astype(jnp.float32).reshape(seq_rows, head_count, head_size)
    key_heads = key_row.astype(jnp.float32).reshape(
        seq_rows, head_count, head_size
    ) * head_size ** (-0.5)
    value_heads = value_row.astype(jnp.float32).reshape(seq_rows, head_count, head_size)
    log_forget = jax.nn.log_sigmoid(forget_pre)
    new_max = jnp.maximum(log_forget + state_max, input_pre)
    keep_old = jnp.exp(log_forget + state_max - new_max)
    keep_new = jnp.exp(input_pre - new_max)
    new_matrix = (
        keep_old[:, :, None, None] * state_matrix
        + keep_new[:, :, None, None] * value_heads[:, :, :, None] * key_heads[:, :, None, :]
    )
    new_norm = keep_old[:, :, None] * state_norm + keep_new[:, :, None] * key_heads
    numerator = jnp.einsum(
        "bhvd,bhd->bhv", new_matrix, query_heads, precision=lax.Precision.HIGHEST
    )
    denominator = jnp.sum(new_norm * query_heads, axis=-1)
    cell_read = numerator / jnp.maximum(jnp.abs(denominator), jnp.exp(-new_max))[:, :, None]
    centered = cell_read - jnp.mean(cell_read, axis=-1, keepdims=True)
    variance = jnp.mean(centered * centered, axis=-1, keepdims=True)
    scaled_cell = (centered * lax.rsqrt(variance + 1e-06)).reshape(seq_rows, head_count * head_size)
    cell_out = (scaled_cell * head_gain * jax.nn.sigmoid(outgate.astype(jnp.float32))).astype(
        jnp.bfloat16
    )
    return (cell_out, new_matrix, new_norm, new_max)


def body(
    tokens,
    mix_gain,
    w_query,
    w_key,
    w_value,
    w_outgate,
    w_igate,
    w_fgate,
    igate_bias,
    fgate_bias,
    head_gain,
    w_out,
    state_matrix,
    state_norm,
    state_max,
    ffn_gain,
    w_expert_gate,
    w_expert_up,
    w_expert_down,
    routes,
    route_weights,
):
    seq_rows, width = tokens.shape
    normed = rms_scale(tokens, mix_gain).astype(jnp.bfloat16)
    weight_list = (w_query, w_key, w_value, w_outgate, w_igate, w_fgate)
    spread = lax.all_to_all(normed, "ep", split_axis=1, concat_axis=0, tiled=True)
    joined = jnp.concatenate(weight_list, axis=1)
    summed = lax.psum_scatter(
        jnp.dot(spread, joined, preferred_element_type=jnp.float32),
        "ep",
        scatter_dimension=0,
        tiled=True,
    )
    bounds = [0]
    for weight in weight_list:
        bounds.append(bounds[-1] + weight.shape[1])
    projected = tuple(
        (summed[:, bounds[index] : bounds[index + 1]] for index in range(len(weight_list)))
    )
    query = projected[0].astype(jnp.bfloat16)
    key_row = projected[1].astype(jnp.bfloat16)
    value_row = projected[2].astype(jnp.bfloat16)
    outgate = projected[3].astype(jnp.bfloat16)
    input_pre = projected[4] + igate_bias
    forget_pre = projected[5] + fgate_bias
    cell_out, new_matrix, new_norm, new_max = memory_cell(
        query,
        key_row,
        value_row,
        outgate,
        input_pre,
        forget_pre,
        head_gain,
        state_matrix,
        state_norm,
        state_max,
    )
    partial_out = jnp.dot(
        cell_out,
        lax.all_gather(w_out, "ep", axis=1, tiled=True),
        preferred_element_type=jnp.float32,
    )
    attended = lax.psum(partial_out.astype(jnp.bfloat16), "tp").astype(jnp.float32)
    resid = (tokens.astype(jnp.float32) + attended).astype(jnp.bfloat16)
    normed_two = rms_scale(resid, ffn_gain).astype(jnp.bfloat16)
    ep_count = lax.axis_size("ep")
    local_experts = w_expert_gate.shape[0]
    expert_total = local_experts * ep_count
    top_count = routes.shape[1]
    capacity = max(2, 2 * seq_rows * top_count // expert_total)
    flat_routes = routes.reshape(-1)
    onehot = (flat_routes[:, None] == jnp.arange(expert_total, dtype=jnp.int32)[None, :]).astype(
        jnp.int32
    )
    earlier = jnp.cumsum(onehot, axis=0, dtype=jnp.int32) - onehot
    slots = jnp.sum(onehot * earlier, axis=1, dtype=jnp.int32)
    targets = flat_routes * capacity + slots
    dispatch = (
        targets[:, None] == jnp.arange(expert_total * capacity, dtype=jnp.int32)[None, :]
    ).astype(jnp.bfloat16)
    route_rows = jnp.repeat(normed_two, top_count, axis=0)
    outgoing = jnp.einsum(
        "rs,rd->sd", dispatch, route_rows, preferred_element_type=jnp.float32
    ).astype(jnp.bfloat16)
    outgoing = outgoing.reshape(expert_total, capacity, width)
    received = lax.all_to_all(outgoing, "ep", split_axis=0, concat_axis=0, tiled=True)
    slot_count = received.shape[1]
    regrouped = received.reshape(ep_count, local_experts, slot_count, width)
    gate_pre = jnp.einsum(
        "nxcd,xdf->nxcf", regrouped, w_expert_gate, preferred_element_type=jnp.float32
    )
    up_pre = jnp.einsum(
        "nxcd,xdf->nxcf", regrouped, w_expert_up, preferred_element_type=jnp.float32
    )
    hidden = (jax.nn.silu(gate_pre) * up_pre).astype(jnp.bfloat16)
    partial_down = jnp.einsum(
        "nxcf,xfd->nxcd", hidden, w_expert_down, preferred_element_type=jnp.float32
    )
    expert_sum = lax.psum(partial_down.astype(jnp.bfloat16), "tp")
    finished = expert_sum.reshape(ep_count * local_experts, slot_count, width)
    returned = lax.all_to_all(finished, "ep", split_axis=0, concat_axis=0, tiled=True)
    picked = jnp.dot(
        dispatch,
        returned.reshape(expert_total * capacity, width),
        preferred_element_type=jnp.float32,
    )
    weighted = jnp.sum(
        picked.reshape(seq_rows, top_count, width) * route_weights[:, :, None], axis=1
    )
    mixed = (resid.astype(jnp.float32) + weighted).astype(jnp.bfloat16)
    return (mixed, new_matrix, new_norm, new_max)


def solution(mesh):
    placed = (
        P("ep", None),
        P(),
        P("ep", "tp"),
        P("ep", "tp"),
        P("ep", "tp"),
        P("ep", "tp"),
        P("ep", "tp"),
        P("ep", "tp"),
        P("tp"),
        P("tp"),
        P("tp"),
        P("tp", "ep"),
        P("ep", "tp", None, None),
        P("ep", "tp", None),
        P("ep", "tp"),
        P(),
        P("ep", None, "tp"),
        P("ep", None, "tp"),
        P("ep", "tp", None),
        P("ep", None),
        P("ep", None),
    )
    return jax.shard_map(
        body,
        mesh=mesh,
        in_specs=placed,
        out_specs=(P("ep", None), P("ep", "tp", None, None), P("ep", "tp", None), P("ep", "tp")),
        check_vma=False,
    )
```

profile of v0, /device:TPU:0, one launch (start us, length us, event | category | flops | bytes accessed | tf_op | source)
XLA Modules:
  0.0 341.9 jit_solution(8380659892496630698)
XLA Ops:
  7.2 1.2 fusion.36
  8.4 1.7 copy_bitcast_fusion
  10.1 8.3 %all-to-all-start = ((bf16[32,16,128]{2,0,1:T(8,128)(2,1)}), bf16[32,16,128]{2,0,1:T(8,128)(2,1)S(1)}, u32[]{:S(2)}, u32[]{:S(2)}) async-start(bf16[32,16,128]{2,0,1:T(8,128)(2,1)} %copy_bitcast_fusion), calls=%async_computation | async-start | bytes 262144 | tf_op jit(solution)/shard_map/all_to_all | solution.py:82
  21.1 5.1 %all-to-all-done = bf16[32,16,128]{2,0,1:T(8,128)(2,1)S(1)} async-done(((bf16[32,16,128]{2,0,1:T(8,128)(2,1)}), bf16[32,16,128]{2,0,1:T(8,128)(2,1)S(1)}, u32[]{:S(2)}, u32[]{:S(2)}) %all-to-all-start) | async-done | bytes 131104 | tf_op jit(solution)/shard_map/all_to_all | solution.py:82
  26.2 1.9 fusion.62
  29.6 125.3 %reduce-scatter.2.cloned.1.call-done = f32[32,1032]{1,0:T(8,128)} async-done(((f32[512,1032]{1,0:T(8,128)}), f32[32,1032]{1,0:T(8,128)}) %reduce-scatter.2.cloned.1.call-update) | async-done | bytes 132112 | tf_op jit(solution)/shard_map/reduce_scatter | solution.py:84
  158.8 3.8 %multiply_add_fusion = f32[32,4,64,64]{3,2,1,0:T(8,128)S(1)} fusion(f32[32,4,64,64]{3,2,1,0:T(8,128)} %param.33, f32[32,4,64]{2,1,0:T(4,128)S(1)} %get-tuple-element.30, f32[32,4,64]{2,1,0:T(4,128)S(1)} %get-tuple-element.31, f32[32,4]{1,0:T(8,128)S(1)} %subtract_exponential_fusion.1), kind=kLoop, calls=%fused_computation | loop fusion | flops 1572864 | bytes 4260352 | tf_op jit(solution)/shard_map/add | solution.py:38
  162.6 2.0 copy-done.1
  164.6 3.4 fusion.63
  168.6 39.4 %all-gather.2.cloned.1.call-done = bf16[256,2048]{1,0:T(8,128)(2,1)} async-done(((bf16[256,128]{1,0:T(8,128)(2,1)}), bf16[256,2048]{1,0:T(8,128)(2,1)}) %all-gather.2.cloned.1.call-update) | async-done | bytes 1048592 | tf_op jit(solution)/shard_map/all_gather | solution.py:116
  208.0 2.2 convolution_convert_fusion.1
  210.7 17.1 %all-reduce.3.cloned.1.call-done = bf16[32,2048]{1,0:T(8,128)(2,1)} async-done(((bf16[32,2048]{1,0:T(8,128)(2,1)}), bf16[32,2048]{1,0:T(8,128)(2,1)}) %all-reduce.3.cloned.1.call-update) | async-done | bytes 131088 | tf_op jit(solution)/shard_map/psum | solution.py:119
  230.1 1.1 reshape.153
  231.2 2.4 convolution_convert_fusion
  233.6 2.1 reshape.154
  235.7 33.5 %all_to_all.29 = bf16[16,12,2048]{2,1,0:T(8,128)(2,1)S(1)} all-to-all(bf16[16,12,2048]{2,1,0:T(8,128)(2,1)} %reshape.154), channel_id=1, replica_groups=mesh['ep'=16,'tp'=2] {'ep'}, dimensions={0} | all-to-all | bytes 1572864 | tf_op jit(solution)/shard_map/all_to_all | solution.py:142
  270.2 3.8 %fusion.9 = f32[16,1,12,704]{3,0,2,1:T(8,128)} fusion(bf16[1,2048,704]{1,2,0:T(8,128)(2,1)} %param.37, bf16[16,12,2048]{2,1,0:T(8,128)(2,1)S(1)} %all_to_all.29), kind=kOutput, calls=%fused_computation.11 | convolution fusion | flops 553648128 | bytes 4210688 | tf_op jit(solution)/shard_map/nxcd,xdf->nxcf/dot_general | solution.py:145
  274.1 5.2 %fusion.6 = bf16[16,12,2048]{2,0,1:T(8,128)(2,1)} fusion(bf16[1,704,2048]{2,1,0:T(8,128)(2,1)S(1)} %copy-done, bf16[1,2048,704]{1,2,0:T(8,128)(2,1)} %param.38, f32[16,1,12,704]{3,0,2,1:T(8,128)} %fusion.9, bf16[16,12,2048]{2,1,0:T(8,128)(2,1)} %copy-done.4), kind=kOutput, calls=%fused_computation.7 | convolution fusion | flops 1108500480 | bytes 7880704 | tf_op jit(solution)/shard_map/nxcf,xfd->nxcd/dot_general | solution.py:152
  279.3 17.5 %all-reduce.5.cloned.1.call-done = bf16[16,12,2048]{2,0,1:T(8,128)(2,1)} async-done(((bf16[16,12,2048]{2,0,1:T(8,128)(2,1)}), bf16[16,12,2048]{2,0,1:T(8,128)(2,1)}) %all-reduce.5.cloned.1.call-update) | async-done | bytes 786448 | tf_op jit(solution)/shard_map/psum | solution.py:155
  296.7 2.6 copy.65
  299.3 7.0 %all-to-all-start.2 = ((bf16[16,12,2048]{2,1,0:T(8,128)(2,1)}), bf16[16,12,2048]{2,1,0:T(8,128)(2,1)}, u32[]{:S(2)}, u32[]{:S(2)}) async-start(bf16[16,12,2048]{2,1,0:T(8,128)(2,1)} %copy.65), calls=%async_computation.3 | async-start | bytes 2097152 | tf_op jit(solution)/shard_map/all_to_all | solution.py:157
  307.2 23.8 %all-to-all-done.2 = bf16[16,12,2048]{2,1,0:T(8,128)(2,1)} async-done(((bf16[16,12,2048]{2,1,0:T(8,128)(2,1)}), bf16[16,12,2048]{2,1,0:T(8,128)(2,1)}, u32[]{:S(2)}, u32[]{:S(2)}) %all-to-all-start.2) | async-done | bytes 786464 | tf_op jit(solution)/shard_map/all_to_all | solution.py:157
  331.1 2.1 reshape.169
  333.2 1.5 fusion.18
  (75 shorter events, 14.1 us)
Async XLA Ops:
  7.2 266.9 %copy-start = (bf16[1,704,2048]{2,1,0:T(8,128)(2,1)S(1)}, bf16[1,704,2048]{2,1,0:T(8,128)(2,1)}, u32[]{:S(2)}) copy-start(bf16[1,704,2048]{2,1,0:T(8,128)(2,1)} %param.39) | copy-start | bytes 8650756
  10.1 16.1 %all-to-all-start = ((bf16[32,16,128]{2,0,1:T(8,128)(2,1)}), bf16[32,16,128]{2,0,1:T(8,128)(2,1)S(1)}, u32[]{:S(2)}, u32[]{:S(2)}) async-start(bf16[32,16,128]{2,0,1:T(8,128)(2,1)} %copy_bitcast_fusion), calls=%async_computation | async-start | bytes 262144 | tf_op jit(solution)/shard_map/all_to_all | solution.py:82
  18.4 136.5 %reduce-scatter.2.cloned.1.call-start = ((), (), s32[]{:S(2)}) async-start(), calls=%async_computation.4 | async-start | bytes 2506752 | tf_op jit(solution)/shard_map/reduce_scatter | solution.py:84
  20.1 8.8 %copy-start.13 = (f32[32,4]{0,1:T(4,128)S(1)}, f32[32,4]{0,1:T(4,128)}, u32[]{:S(2)}) copy-start(f32[32,4]{0,1:T(4,128)} %param.35) | copy-start | bytes 1540
  20.1 8.9 %copy-start.7 = (s32[32,3]{0,1:T(4,128)S(1)}, s32[32,3]{0,1:T(4,128)}, u32[]{:S(2)}) copy-start(s32[32,3]{0,1:T(4,128)} %param.40) | copy-start | bytes 1156
  26.2 130.0 %copy-start.10 = (f32[4]{0:T(128)S(1)}, f32[4]{0:T(128)}, u32[]{:S(2)}) copy-start(f32[4]{0:T(128)} %param.30) | copy-start | bytes 52
  26.2 130.0 %copy-start.15 = (f32[4]{0:T(128)S(1)}, f32[4]{0:T(128)}, u32[]{:S(2)}) copy-start(f32[4]{0:T(128)} %param.29) | copy-start | bytes 52
  26.2 131.8 %copy-start.5 = (f32[32,4,64]{2,1,0:T(4,128)S(1)}, f32[32,4,64]{2,1,0:T(4,128)}, u32[]{:S(2)}) copy-start(f32[32,4,64]{2,1,0:T(4,128)} %param.34) | copy-start | bytes 98308
  28.1 179.9 %all-gather.2.cloned.1.call-start = ((), (), s32[]{:S(2)}) async-start(), calls=%async_computation.5 | async-start | bytes 1114112 | tf_op jit(solution)/shard_map/all_gather | solution.py:116
  28.8 199.0 %all-reduce.3.cloned.1.call-start = ((), (), s32[]{:S(2)}) async-start(), calls=%async_computation.6 | async-start | bytes 262144 | tf_op jit(solution)/shard_map/psum | solution.py:119
  29.6 180.6 %copy-start.11 = (s32[96]{0:T(128)}, s32[96]{0:T(128)S(1)}, u32[]{:S(2)}) copy-start(s32[96]{0:T(128)S(1)} %select_reduce_fusion) | copy-start | bytes 1156
  162.6 2.0 copy-start.1
  164.6 43.4 %copy-start.14 = (f32[256]{0:T(256)S(1)}, f32[256]{0:T(256)}, u32[]{:S(2)}) copy-start(f32[256]{0:T(256)} %param.31) | copy-start | bytes 3076
  164.6 63.2 %copy-start.2 = (bf16[32,2048]{1,0:T(8,128)(2,1)S(1)}, bf16[32,2048]{1,0:T(8,128)(2,1)}, u32[]{:S(2)}) copy-start(bf16[32,2048]{1,0:T(8,128)(2,1)} %param.21) | copy-start | bytes 393220
  164.6 64.3 %copy-start.6 = (f32[2048]{0:T(1024)S(1)}, f32[2048]{0:T(1024)}, u32[]{:S(2)}) copy-start(f32[2048]{0:T(1024)} %param.36) | copy-start | bytes 24580
  210.1 86.6 %all-reduce.5.cloned.1.call-start = ((), (), s32[]{:S(2)}) async-start(), calls=%async_computation.7 | async-start | bytes 1572864 | tf_op jit(solution)/shard_map/psum | solution.py:155
  269.3 1.0 copy-start.4
  279.2 27.1 %copy-start.12 = (s32[96]{0:T(128)S(1)}, s32[96]{0:T(128)}, u32[]{:S(2)}) copy-start(s32[96]{0:T(128)} %copy-done.11) | copy-start | bytes 1156
  279.3 27.3 %copy-start.8 = (s32[32,3]{0,1:T(4,128)S(1)}, s32[32,3]{0,1:T(4,128)}, u32[]{:S(2)}) copy-start(s32[32,3]{0,1:T(4,128)} %param.40) | copy-start | bytes 1156
  279.3 53.9 %copy-start.9 = (f32[32,3]{0,1:T(4,128)S(1)}, f32[32,3]{0,1:T(4,128)}, u32[]{:S(2)}) copy-start(f32[32,3]{0,1:T(4,128)} %param.41) | copy-start | bytes 1156
  299.3 35.3 %copy-start.3 = (bf16[32,2048]{1,0:T(8,128)(2,1)S(1)}, bf16[32,2048]{1,0:T(8,128)(2,1)}, u32[]{:S(2)}) copy-start(bf16[32,2048]{1,0:T(8,128)(2,1)} %all-reduce.3.cloned.1.call-done) | copy-start | bytes 393220
  299.3 31.7 %all-to-all-start.2 = ((bf16[16,12,2048]{2,1,0:T(8,128)(2,1)}), bf16[16,12,2048]{2,1,0:T(8,128)(2,1)}, u32[]{:S(2)}, u32[]{:S(2)}) async-start(bf16[16,12,2048]{2,1,0:T(8,128)(2,1)} %copy.65), calls=%async_computation.3 | async-start | bytes 2097152 | tf_op jit(solution)/shard_map/all_to_all | solution.py:157
Sparse Core Ops, SparseCore 0:
  28.2 126.6 reduce-scatter.1
  157.6 50.2 all-gather.1
  210.8 16.9 all-reduce.2
  279.4 17.2 all-reduce.4
where the time goes:
time: 343 us; the launch traced here: 342 us
  waiting for transfers between devices  229 us (67%)
  blocking collectives  33.5 us (10%)
  matrix products  20.3 us (6%)
  starting transfers between devices  15.5 us (5%)
  local copies, waits for them, and re-layouts  15.4 us (4%)
  other arithmetic  14.3 us (4%)
  between operations  14 us (4%)
    reduce_scatter x1, waiting for transfers between devices, body(): lax.psum_scatter(jnp.dot(spread, joined, preferred_element_type=jnp.float...  125 us
    all_gather x1, waiting for transfers between devices, body(): lax.all_gather(w_out, 'ep', axis=1, tiled=True)  39.4 us
    all_to_all x1, blocking collectives, body(): lax.all_to_all(outgoing, 'ep', split_axis=0, concat_axis=0, tiled=True)  33.5 us
    all_to_all x1, waiting for transfers between devices, body(): lax.all_to_all(finished, 'ep', split_axis=0, concat_axis=0, tiled=True)  23.8 us
    psum x1, waiting for transfers between devices, body(): expert_sum = lax.psum(partial_down.astype(jnp.bfloat16), 'tp')  17.5 us
    psum x1, waiting for transfers between devices, body(): lax.psum(partial_out.astype(jnp.bfloat16), 'tp').astype(jnp.float32)  17.1 us
    all_to_all x1, starting transfers between devices, body(): lax.all_to_all(normed, 'ep', split_axis=1, concat_axis=0, tiled=True)  8.34 us
    all_to_all x1, starting transfers between devices, body(): lax.all_to_all(finished, 'ep', split_axis=0, concat_axis=0, tiled=True)  7.01 us
  transfers between devices with their start and end apart: 6, of which 6 were waited for; matrix products, arithmetic and copies ran while one was open for 5% of the time, Pallas kernels for 0%

commit v1 on v0

v1 whole, which is shorter than its diff:
```python
import jax
import jax.numpy as jnp
from jax import lax
from jax.sharding import PartitionSpec as P


def rms_scale(values_in, gain_vec):
    widened = values_in.astype(jnp.float32)
    return (
        widened * lax.rsqrt(jnp.mean(widened * widened, axis=-1, keepdims=True) + 1e-06) * gain_vec
    )


def memory_cell(
    query,
    key_row,
    value_row,
    outgate,
    input_pre,
    forget_pre,
    head_gain,
    state_matrix,
    state_norm,
    state_max,
):
    seq_rows, head_count = input_pre.shape
    head_size = query.shape[1] // head_count
    query_heads = query.astype(jnp.float32).reshape(seq_rows, head_count, head_size)
    key_heads = key_row.astype(jnp.float32).reshape(
        seq_rows, head_count, head_size
    ) * head_size ** (-0.5)
    value_heads = value_row.astype(jnp.float32).reshape(seq_rows, head_count, head_size)
    log_forget = jax.nn.log_sigmoid(forget_pre)
    new_max = jnp.maximum(log_forget + state_max, input_pre)
    keep_old = jnp.exp(log_forget + state_max - new_max)
    keep_new = jnp.exp(input_pre - new_max)
    new_matrix = (
        keep_old[:, :, None, None] * state_matrix
        + keep_new[:, :, None, None] * value_heads[:, :, :, None] * key_heads[:, :, None, :]
    )
    new_norm = keep_old[:, :, None] * state_norm + keep_new[:, :, None] * key_heads
    numerator = jnp.einsum(
        "bhvd,bhd->bhv", new_matrix, query_heads, precision=lax.Precision.HIGHEST
    )
    denominator = jnp.sum(new_norm * query_heads, axis=-1)
    cell_read = numerator / jnp.maximum(jnp.abs(denominator), jnp.exp(-new_max))[:, :, None]
    centered = cell_read - jnp.mean(cell_read, axis=-1, keepdims=True)
    variance = jnp.mean(centered * centered, axis=-1, keepdims=True)
    scaled_cell = (centered * lax.rsqrt(variance + 1e-06)).reshape(seq_rows, head_count * head_size)
    cell_out = (scaled_cell * head_gain * jax.nn.sigmoid(outgate.astype(jnp.float32))).astype(
        jnp.bfloat16
    )
    return (cell_out, new_matrix, new_norm, new_max)


def torus_factors(count):
    side = 1
    while (2 * side) ** 3 <= count:
        side *= 2
    while count % (side * side):
        side -= 1
    return (count // (side * side), side, side)


def shift_pairs(factors, axis, step):
    pairs = []
    inner = 1
    for size in factors[axis + 1 :]:
        inner *= size
    total = factors[0] * factors[1] * factors[2]
    for source in range(total):
        place = source // inner % factors[axis]
        pairs.append((source, source + ((place + step) % factors[axis] - place) * inner))
    return pairs


def own_place(factors, axis):
    inner = 1
    for size in factors[axis + 1 :]:
        inner *= size
    return lax.axis_index("ep") // inner % factors[axis]


def reduce_stage(parts, factors, axis, dim):
    size = factors[axis]
    place = own_place(factors, axis)
    total = lax.dynamic_index_in_dim(parts, place, dim, keepdims=True).astype(jnp.float32)
    for step in range(1, size):
        sent = lax.dynamic_index_in_dim(parts, (place + step) % size, dim, keepdims=True)
        total = total + lax.ppermute(
            sent.astype(jnp.bfloat16), "ep", shift_pairs(factors, axis, step)
        ).astype(jnp.float32)
    return total


def staged_reduce_scatter(partial, factors, order):
    rows = partial.shape[0] // (factors[0] * factors[1] * factors[2])
    parts = partial.reshape(*factors, rows, partial.shape[1])
    for axis in order:
        parts = reduce_stage(parts, factors, axis, axis)
    return parts.reshape(rows, partial.shape[1])


def swap_cores(values_in):
    return lax.ppermute(values_in, "tp", [(0, 1), (1, 0)])


def body(
    tokens,
    mix_gain,
    w_query,
    w_key,
    w_value,
    w_outgate,
    w_igate,
    w_fgate,
    igate_bias,
    fgate_bias,
    head_gain,
    w_out,
    state_matrix,
    state_norm,
    state_max,
    ffn_gain,
    w_expert_gate,
    w_expert_up,
    w_expert_down,
    routes,
    route_weights,
):
    seq_rows, width = tokens.shape
    ep_count = lax.axis_size("ep")
    factors = torus_factors(ep_count)
    w_out_full = lax.all_gather(w_out, "ep", axis=1, tiled=True)

    local_experts = w_expert_gate.shape[0]
    expert_total = local_experts * ep_count
    top_count = routes.shape[1]
    capacity = max(2, 2 * seq_rows * top_count // expert_total)
    core_slots = -(-((capacity + 1) // 2) // 8) * 8
    core = lax.axis_index("tp")
    flat_routes = routes.reshape(-1)
    onehot = (flat_routes[:, None] == jnp.arange(expert_total, dtype=jnp.int32)[None, :]).astype(
        jnp.int32
    )
    earlier = jnp.cumsum(onehot, axis=0, dtype=jnp.int32) - onehot
    slots = jnp.sum(onehot * earlier, axis=1, dtype=jnp.int32)
    targets = jnp.where(slots % 2 == core, flat_routes * core_slots + slots // 2, -1)
    places = jnp.arange(expert_total * core_slots, dtype=jnp.int32)
    hits = (targets[:, None] == places[None, :]).reshape(seq_rows, top_count, -1)
    token_hits = jnp.any(hits, axis=1).astype(jnp.bfloat16)
    weight_hits = jnp.sum(jnp.where(hits, route_weights[:, :, None], 0.0), axis=1)

    normed = rms_scale(tokens, mix_gain).astype(jnp.bfloat16)
    spread = lax.all_to_all(normed, "ep", split_axis=1, concat_axis=0, tiled=True)
    first_list = (w_query, w_key)
    second_list = (w_value, w_outgate, w_igate, w_fgate)
    first = staged_reduce_scatter(
        jnp.dot(
            spread, jnp.concatenate(first_list, axis=1), preferred_element_type=jnp.float32
        ).astype(jnp.bfloat16),
        factors,
        (2, 1, 0),
    )
    second = staged_reduce_scatter(
        jnp.dot(
            spread, jnp.concatenate(second_list, axis=1), preferred_element_type=jnp.float32
        ).astype(jnp.bfloat16),
        factors,
        (1, 2, 0),
    )
    head_width = w_query.shape[1]
    head_count = w_igate.shape[1]
    query = first[:, :head_width].astype(jnp.bfloat16)
    key_row = first[:, head_width:].astype(jnp.bfloat16)
    value_row = second[:, :head_width].astype(jnp.bfloat16)
    outgate = second[:, head_width : 2 * head_width].astype(jnp.bfloat16)
    input_pre = second[:, 2 * head_width : 2 * head_width + head_count] + igate_bias
    forget_pre = second[:, 2 * head_width + head_count :] + fgate_bias
    cell_out, new_matrix, new_norm, new_max = memory_cell(
        query,
        key_row,
        value_row,
        outgate,
        input_pre,
        forget_pre,
        head_gain,
        state_matrix,
        state_norm,
        state_max,
    )
    partial_out = jnp.dot(cell_out, w_out_full, preferred_element_type=jnp.float32).astype(
        jnp.bfloat16
    )
    attended = partial_out.astype(jnp.float32) + swap_cores(partial_out).astype(jnp.float32)
    resid = (tokens.astype(jnp.float32) + attended).astype(jnp.bfloat16)
    normed_two = rms_scale(resid, ffn_gain).astype(jnp.bfloat16)

    outgoing = lax.dot_general(
        token_hits, normed_two, (((0,), (0,)), ((), ())), preferred_element_type=jnp.float32
    ).astype(jnp.bfloat16)
    outgoing = outgoing.reshape(expert_total, core_slots, width)
    received = lax.all_to_all(outgoing, "ep", split_axis=0, concat_axis=0, tiled=True)
    other = swap_cores(received)

    def grouped(rows):
        rows = rows.reshape(ep_count, local_experts, core_slots, width)
        return jnp.swapaxes(rows, 0, 1).reshape(local_experts, ep_count * core_slots, width)

    regrouped = jnp.concatenate([grouped(received), grouped(other)], axis=1)
    gate_pre = jnp.einsum("xcd,xdf->xcf", regrouped, w_expert_gate, preferred_element_type=jnp.float32)
    up_pre = jnp.einsum("xcd,xdf->xcf", regrouped, w_expert_up, preferred_element_type=jnp.float32)
    hidden = (jax.nn.silu(gate_pre) * up_pre).astype(jnp.bfloat16)
    partial_down = jnp.einsum(
        "xcf,xfd->xcd", hidden, w_expert_down, preferred_element_type=jnp.float32
    ).astype(jnp.bfloat16)
    half = ep_count * core_slots
    expert_sum = (
        partial_down[:, :half].astype(jnp.float32)
        + swap_cores(partial_down[:, half:]).astype(jnp.float32)
    ).astype(jnp.bfloat16)
    finished = jnp.swapaxes(
        expert_sum.reshape(local_experts, ep_count, core_slots, width), 0, 1
    ).reshape(ep_count * local_experts, core_slots, width)
    returned = lax.all_to_all(finished, "ep", split_axis=0, concat_axis=0, tiled=True)
    returned = returned.reshape(expert_total * core_slots, width)
    weight_high = weight_hits.astype(jnp.bfloat16)
    weight_rest = weight_hits - weight_high.astype(jnp.float32)
    weight_low = weight_rest.astype(jnp.bfloat16)
    weighted = jnp.dot(weight_high, returned, preferred_element_type=jnp.float32) + jnp.dot(
        weight_low, returned, preferred_element_type=jnp.float32
    )
    weighted = weighted + swap_cores(weighted)
    mixed = (resid.astype(jnp.float32) + weighted).astype(jnp.bfloat16)
    return (mixed, new_matrix, new_norm, new_max)


def solution(mesh):
    placed = (
        P("ep", None),
        P(),
        P("ep", "tp"),
        P("ep", "tp"),
        P("ep", "tp"),
        P("ep", "tp"),
        P("ep", "tp"),
        P("ep", "tp"),
        P("tp"),
        P("tp"),
        P("tp"),
        P("tp", "ep"),
        P("ep", "tp", None, None),
        P("ep", "tp", None),
        P("ep", "tp"),
        P(),
        P("ep", None, "tp"),
        P("ep", None, "tp"),
        P("ep", "tp", None),
        P("ep", None),
        P("ep", None),
    )
    return jax.shard_map(
        body,
        mesh=mesh,
        in_specs=placed,
        out_specs=(P("ep", None), P("ep", "tp", None, None), P("ep", "tp", None), P("ep", "tp")),
        check_vma=False,
    )
```

time: 343 us -> 147 us (0.43)
  waiting for transfers between devices: 229 us -> 36.2 us
  blocking collectives: 33.5 us -> 19.9 us
  starting transfers between devices: 15.5 us -> 24.4 us
  other arithmetic: 14.3 us -> 18.2 us
    reduce_scatter x1 -> x0, waiting for transfers between devices: 125 us -> none  [body(): lax.psum_scatter(jnp.dot(spread, joined, preferred_element_type=jnp.float...]
    all_gather x1, waiting for transfers between devices: 39.4 us -> 0.01 us  [body(): w_out_full = lax.all_gather(w_out, 'ep', axis=1, tiled=True)]
    psum x2 -> x0, waiting for transfers between devices: 34.5 us -> none  [the longest x1 17.5 us: body(): expert_sum = lax.psum(partial_down.astype(jnp.bfloat16), 'tp')]
    ppermute x0 -> x14, waiting for transfers between devices: none -> 18.9 us  [the longest x10 13 us: reduce_stage(): lax.ppermute(sent.astype(jnp.bfloat16), 'ep', shift_pairs(factors, axis,...]
    all_to_all x1, blocking collectives: 33.5 us -> 19.9 us  [body(): lax.all_to_all(outgoing, 'ep', split_axis=0, concat_axis=0, tiled=True)]
    ppermute x0 -> x14, starting transfers between devices: none -> 12 us  [the longest x10 11.8 us: reduce_stage(): lax.ppermute(sent.astype(jnp.bfloat16), 'ep', shift_pairs(factors, axis,...]
    all_to_all x1, waiting for transfers between devices: 23.8 us -> 14 us  [body(): lax.all_to_all(finished, 'ep', split_axis=0, concat_axis=0, tiled=True)]
    reshape x3 -> x0, local copies, waits for them, and re-layouts: 5.32 us -> none  [the longest x1 2.12 us: body(): outgoing = outgoing.reshape(expert_total, capacity, width)]
  transfers between devices with their start and end apart: 6 -> 17, of which waited for: 6 -> 12; matrix products, arithmetic and copies ran while one was open for 5% -> 20% of each run, Pallas kernels for 0% -> 0%
where the time goes in v1:
time: 147 us; the launch traced here: 146 us
  waiting for transfers between devices  36.2 us (25%)
  starting transfers between devices  24.4 us (17%)
  blocking collectives  19.9 us (14%)
  matrix products  19.4 us (13%)
  other arithmetic  18.2 us (12%)
  between operations  14.5 us (10%)
  local copies, waits for them, and re-layouts  13.2 us (9%)
    all_to_all x1, blocking collectives, body(): lax.all_to_all(outgoing, 'ep', split_axis=0, concat_axis=0, tiled=True)  19.9 us
    all_to_all x1, waiting for transfers between devices, body(): lax.all_to_all(finished, 'ep', split_axis=0, concat_axis=0, tiled=True)  14 us
    ppermute x10, waiting for transfers between devices, reduce_stage(): lax.ppermute(sent.astype(jnp.bfloat16), 'ep', shift_pairs(factors, axis,...  13 us
    ppermute x10, starting transfers between devices, reduce_stage(): lax.ppermute(sent.astype(jnp.bfloat16), 'ep', shift_pairs(factors, axis,...  11.8 us
    all_to_all x1, starting transfers between devices, body(): lax.all_to_all(normed, 'ep', split_axis=1, concat_axis=0, tiled=True)  8.34 us
    unnamed x29, local copies, waits for them, and re-layouts  7.86 us
    dot_general x1, matrix products, body(): jnp.einsum('xcf,xfd->xcd', hidden, w_expert_down, preferred_element_type=...  6.41 us
    ppermute x4, waiting for transfers between devices, swap_cores(): return lax.ppermute(values_in, 'tp', [(0, 1), (1, 0)])  5.97 us
  transfers between devices with their start and end apart: 17, of which 12 were waited for; matrix products, arithmetic and copies ran while one was open for 20% of the time, Pallas kernels for 0%

profile of v1, /device:TPU:0, one launch (start us, length us, event | category | flops | bytes accessed | tf_op | source)
XLA Modules:
  0.0 145.8 jit_solution(4890055975941566926)
XLA Ops:
  9.1 1.7 %copy_bitcast_fusion = bf16[32,16,128]{2,0,1:T(8,128)(2,1)} fusion(bf16[32,2048]{1,0:T(8,128)(2,1)} %param.21, f32[2048]{0:T(1024)} %param.22, f32[32]{0:T(128)S(1)} %add_rsqrt_fusion.2), kind=kLoop, calls=%fused_computation.55 | loop fusion | flops 262144 | bytes 270464 | tf_op jit(solution)/shard_map/all_to_all | solution.py:155
  10.8 8.3 %all-to-all-start = ((bf16[32,16,128]{2,0,1:T(8,128)(2,1)}), bf16[32,16,128]{2,0,1:T(8,128)(2,1)S(1)}, u32[]{:S(2)}, u32[]{:S(2)}) async-start(bf16[32,16,128]{2,0,1:T(8,128)(2,1)} %copy_bitcast_fusion), calls=%async_computation | async-start | bytes 262144 | tf_op jit(solution)/shard_map/all_to_all | solution.py:155
  24.3 2.6 %all-to-all-done = bf16[32,16,128]{2,0,1:T(8,128)(2,1)S(1)} async-done(((bf16[32,16,128]{2,0,1:T(8,128)(2,1)}), bf16[32,16,128]{2,0,1:T(8,128)(2,1)S(1)}, u32[]{:S(2)}, u32[]{:S(2)}) %all-to-all-start) | async-done | bytes 131104 | tf_op jit(solution)/shard_map/all_to_all | solution.py:155
  30.0 2.0 %convolution_convert_fusion.2 = bf16[512,520]{0,1:T(8,128)(2,1)} fusion(bf16[512,128]{1,0:T(8,128)(2,1)S(1)} %bitcast.65, bf16[128,4]{1,0:T(8,128)(2,1)S(1)} %copy.59, bf16[128,4]{1,0:T(8,128)(2,1)S(1)} %copy.58, bf16[128,256]{1,0:T(8,128)(2,1)} %param.26, bf16[128,256]{1,0:T(8,128)(2,1)} %param.25), kind=kOutput, calls=%fused_computation.13 | convolution fusion | flops 68956160 | bytes 796672 | tf_op jit(solution)/shard_map/dot_general | solution.py:166
  33.7 2.2 %collective-permute-done.5 = bf16[4,2,1,32,512]{4,3,2,1,0:T(8,128)(2,1)} collective-permute-done((bf16[4,2,1,32,512]{4,3,2,1,0:T(8,128)(2,1)}, bf16[4,2,1,32,512]{4,3,2,1,0:T(8,128)(2,1)}, u32[]{:S(2)}, u32[]{:S(2)}) %collective-permute-start.5) | collective-permute-done | bytes 262176 | tf_op jit(solution)/shard_map/ppermute | solution.py:90
  38.0 6.3 %collective-permute-done = bf16[4,1,2,32,520]{4,3,2,1,0:T(8,128)(2,1)S(1)} collective-permute-done((bf16[4,1,2,32,520]{4,3,2,1,0:T(8,128)(2,1)S(1)}, bf16[4,1,2,32,520]{4,3,2,1,0:T(8,128)(2,1)S(1)}, u32[]{:S(2)}, u32[]{:S(2)}) %collective-permute-start) | collective-permute-done | bytes 266272 | tf_op jit(solution)/shard_map/ppermute | solution.py:90
  46.1 3.5 %collective-permute-start.9 = (bf16[1,1,1,32,512]{4,3,2,1,0:T(8,128)(2,1)S(1)}, bf16[1,1,1,32,512]{4,3,2,1,0:T(8,128)(2,1)S(1)}, u32[]{:S(2)}, u32[]{:S(2)}) collective-permute-start(bf16[1,1,1,32,512]{4,3,2,1,0:T(8,128)(2,1)S(1)} %get-tuple-element.31), channel_id=1, source_target_pairs={{0,24},{2,26},{4,28},{6,30},{8,0},{10,2},{12,4},{14,6},{16,8},{18,... | collective-permute-start | bytes 98312 | tf_op jit(solution)/shard_map/ppermute | solution.py:90
  51.0 3.3 %collective-permute-start.4 = (bf16[1,1,1,32,520]{4,3,2,1,0:T(8,128)(2,1)}, bf16[1,1,1,32,520]{4,3,2,1,0:T(8,128)(2,1)S(1)}, u32[]{:S(2)}, u32[]{:S(2)}) collective-permute-start(bf16[1,1,1,32,520]{4,3,2,1,0:T(8,128)(2,1)} %get-tuple-element.28), channel_id=1, source_target_pairs={{0,24},{2,26},{4,28},{6,30},{8,0},{10,2},{12,4},{14,6},{16,8},{18,... | collective-permute-start | bytes 99848 | tf_op jit(solution)/shard_map/ppermute | solution.py:90
  55.6 1.6 %collective-permute-done.2 = bf16[1,1,1,32,520]{4,3,2,1,0:T(8,128)(2,1)S(1)} collective-permute-done((bf16[1,1,1,32,520]{4,3,2,1,0:T(8,128)(2,1)}, bf16[1,1,1,32,520]{4,3,2,1,0:T(8,128)(2,1)S(1)}, u32[]{:S(2)}, u32[]{:S(2)}) %collective-permute-start.2) | collective-permute-done | bytes 33312 | tf_op jit(solution)/shard_map/ppermute | solution.py:90
  57.9 2.1 %collective-permute-done.3 = bf16[1,1,1,32,520]{4,3,2,1,0:T(8,128)(2,1)} collective-permute-done((bf16[1,1,1,32,520]{4,3,2,1,0:T(8,128)(2,1)S(1)}, bf16[1,1,1,32,520]{4,3,2,1,0:T(8,128)(2,1)}, u32[]{:S(2)}, u32[]{:S(2)}) %collective-permute-start.3) | collective-permute-done | bytes 33312 | tf_op jit(solution)/shard_map/ppermute | solution.py:90
  62.6 1.6 %multiply_reduce_fusion.1 = (f32[32,4]{1,0:T(8,128)S(1)}, f32[32,4,64]{2,1,0:T(4,128)}, f32[32,4,64]{2,1,0:T(4,128)S(1)}, f32[32,4,64]{2,1,0:T(4,128)S(1)}) fusion(bf16[32,4,64]{2,1,0:T(4,128)(2,1)S(1)} %reshape.177, f32[32,4,64]{2,1,0:T(4,128)S(1)} %reshape.189, f32[32,4]{1,0:T(8,128)S(1)} %get-tuple-element.22, f32[32,4,64]{2,1,0:T(4,128)} %param.34, ...), kind=kLoop, calls=%fused_computation.66 | loop fusion | flops 65408 | bytes 215040 | tf_op jit(solution)/shard_map/reduce_sum | solution.py:45
  64.2 3.8 %multiply_add_fusion = f32[32,4,64,64]{3,2,1,0:T(8,128)S(1)} fusion(f32[32,4,64,64]{3,2,1,0:T(8,128)} %param.33, f32[32,4,64]{2,1,0:T(4,128)S(1)} %get-tuple-element.33, f32[32,4,64]{2,1,0:T(4,128)S(1)} %get-tuple-element.36, f32[32,4]{1,0:T(8,128)S(1)} %subtract_exponential_fusion.1), kind=kLoop, calls=%fused_computation | loop fusion | flops 1572864 | bytes 4260352 | tf_op jit(solution)/shard_map/add | solution.py:38
  68.0 2.0 %copy-done.1 = f32[32,4,64,64]{3,2,1,0:T(8,128)} copy-done((f32[32,4,64,64]{3,2,1,0:T(8,128)}, f32[32,4,64,64]{3,2,1,0:T(8,128)S(1)}, u32[]{:S(2)}) %copy-start.1) | copy-done | bytes 2097176
  70.0 3.4 %fusion.80 = f32[32,4,1,64]{3,2,1,0:T(1,128)S(1)} fusion(f32[32,4,64,64]{3,2,1,0:T(8,128)S(1)} %multiply_add_fusion, bf16[32,4,64,1]{2,3,1,0:T(2,128)(2,1)S(1)} %reshape.193), kind=kOutput, calls=%fused_computation.129 | convolution fusion | flops 6291456 | bytes 2146304 | tf_op jit(solution)/shard_map/bhvd,bhd->bhv/dot_general | solution.py:42
  77.6 19.9 %all_to_all.29 = bf16[16,8,2048]{2,1,0:T(8,128)(2,1)S(1)} all-to-all(bf16[16,8,2048]{2,1,0:T(8,128)(2,1)S(1)} %fusion.12), channel_id=1, replica_groups=mesh['ep'=16,'tp'=2] {'ep'}, dimensions={0} | all-to-all | bytes 1048576 | tf_op jit(solution)/shard_map/all_to_all | solution.py:203
  97.6 1.9 %collective-permute-done.11 = bf16[16,8,2048]{2,1,0:T(8,128)(2,1)S(1)} collective-permute-done((bf16[16,8,2048]{2,1,0:T(8,128)(2,1)S(1)}, bf16[16,8,2048]{2,1,0:T(8,128)(2,1)S(1)}, u32[]{:S(2)}, u32[]{:S(2)}) %collective-permute-start.11) | collective-permute-done | bytes 524320 | tf_op jit(solution)/shard_map/ppermute | solution.py:105
  100.3 1.9 %fusion.4 = f32[256,704]{0,1:T(8,128)} fusion(bf16[1,2048,704]{1,2,0:T(8,128)(2,1)S(1)} %copy-done.10, bf16[1,128,2048]{2,1,0:T(8,128)(2,1)S(1)} %bitcast.69, bf16[1,128,2048]{2,1,0:T(8,128)(2,1)S(1)} %bitcast.66), kind=kOutput, calls=%fused_computation.5 | convolution fusion | flops 740294656 | bytes 4653056 | tf_op jit(solution)/shard_map/xcd,xdf->xcf/dot_general | solution.py:211
  102.1 6.4 %fusion.9 = bf16[1,256,2048]{2,1,0:T(8,128)(2,1)} fusion(bf16[1,704,2048]{2,1,0:T(8,128)(2,1)S(1)} %copy-done, bf16[1,2048,704]{1,2,0:T(8,128)(2,1)} %param.38, f32[256,704]{0,1:T(8,128)} %fusion.4, bf16[1,128,2048]{2,1,0:T(8,128)(2,1)} %bitcast.70, bf16[1,128,2048]{2,1,0:T(8,128)(2,1)S(1)} %bitcast.67), kind=kOutput, calls=%fused_computation.8 | convolution fusion | flops 1480097792 | bytes 8585216 | tf_op jit(solution)/shard_map/xcf,xfd->xcd/dot_general | solution.py:214
  109.8 1.8 %collective-permute-done.12 = bf16[1,128,2048]{2,1,0:T(8,128)(2,1)S(1)} collective-permute-done((bf16[1,128,2048]{2,1,0:T(8,128)(2,1)S(1)}, bf16[1,128,2048]{2,1,0:T(8,128)(2,1)S(1)}, u32[]{:S(2)}, u32[]{:S(2)}) %collective-permute-start.12) | collective-permute-done | bytes 524320 | tf_op jit(solution)/shard_map/ppermute | solution.py:105
  111.6 2.0 %fusion.24 = bf16[16,8,2048]{2,1,0:T(8,128)(2,1)} fusion(bf16[1,128,2048]{2,1,0:T(8,128)(2,1)S(1)} %collective-permute-done.12, bf16[1,256,2048]{2,1,0:T(8,128)(2,1)} %fusion.9), kind=kLoop, calls=%fused_computation.23 | loop fusion | flops 1048576 | bytes 1572864 | tf_op jit(solution)/shard_map/reshape;transpose;reshape | solution.py:224
  113.6 3.9 %all-to-all-start.2 = ((bf16[16,8,2048]{2,1,0:T(8,128)(2,1)}), bf16[16,8,2048]{2,1,0:T(8,128)(2,1)S(1)}, u32[]{:S(2)}, u32[]{:S(2)}) async-start(bf16[16,8,2048]{2,1,0:T(8,128)(2,1)} %fusion.24), calls=%async_computation.2 | async-start | bytes 1048576 | tf_op jit(solution)/shard_map/all_to_all | solution.py:225
  118.9 14.0 %all-to-all-done.2 = bf16[16,8,2048]{2,1,0:T(8,128)(2,1)S(1)} async-done(((bf16[16,8,2048]{2,1,0:T(8,128)(2,1)}), bf16[16,8,2048]{2,1,0:T(8,128)(2,1)S(1)}, u32[]{:S(2)}, u32[]{:S(2)}) %all-to-all-start.2) | async-done | bytes 524320 | tf_op jit(solution)/shard_map/all_to_all | solution.py:225
  133.8 1.7 %convolution_add_fusion = f32[32,2048]{1,0:T(8,128)} fusion(f32[32,2048]{1,0:T(8,128)S(1)} %fusion.26, bf16[16,8,2048]{2,1,0:T(8,128)(2,1)S(1)} %all-to-all-done.2, f32[32,128]{1,0:T(8,128)} %select_reduce_fusion), kind=kOutput, calls=%fused_computation.11 | convolution fusion | flops 16859136 | bytes 1064960 | tf_op jit(solution)/shard_map/dot_general | solution.py:230
  137.3 1.6 %fusion.36 = bf16[32,2048]{1,0:T(8,128)(2,1)} fusion(bf16[32,2048]{1,0:T(8,128)(2,1)S(1)} %get-tuple-element.17, f32[32,2048]{1,0:T(8,128)} %convolution_add_fusion, f32[32,2048]{1,0:T(8,128)S(1)} %collective-permute-done.13), kind=kLoop, calls=%fused_computation.44 | loop fusion | flops 262144 | bytes 786432 | tf_op jit(solution)/shard_map/convert_element_type | solution.py:234
  (97 shorter events, 31.7 us)
Async XLA Ops:
  7.2 95.0 %copy-start = (bf16[1,704,2048]{2,1,0:T(8,128)(2,1)S(1)}, bf16[1,704,2048]{2,1,0:T(8,128)(2,1)}, u32[]{:S(2)}) copy-start(bf16[1,704,2048]{2,1,0:T(8,128)(2,1)} %param.39) | copy-start | bytes 8650756
  7.2 66.9 %all-gather.2.cloned.1.call-start = ((), (), s32[]{:S(2)}) async-start(), calls=%async_computation.3 | async-start | bytes 1114112 | tf_op jit(solution)/shard_map/all_gather | solution.py:134
  10.8 16.1 %all-to-all-start = ((bf16[32,16,128]{2,0,1:T(8,128)(2,1)}), bf16[32,16,128]{2,0,1:T(8,128)(2,1)S(1)}, u32[]{:S(2)}, u32[]{:S(2)}) async-start(bf16[32,16,128]{2,0,1:T(8,128)(2,1)} %copy_bitcast_fusion), calls=%async_computation | async-start | bytes 262144 | tf_op jit(solution)/shard_map/all_to_all | solution.py:155
  28.9 6.9 %collective-permute-start.5 = (bf16[4,2,1,32,512]{4,3,2,1,0:T(8,128)(2,1)}, bf16[4,2,1,32,512]{4,3,2,1,0:T(8,128)(2,1)}, u32[]{:S(2)}, u32[]{:S(2)}) collective-permute-start(bf16[4,2,1,32,512]{4,3,2,1,0:T(8,128)(2,1)} %constant_dynamic-slice_fusion), channel_id=1, source_target_pairs={{0,2},{2,0},{4,6},{6,4},{8,10},{10,8},{12,14},{14,12},{16,18},{18,... | collective-permute-start | bytes 786440 | tf_op jit(solution)/shard_map/ppermute | solution.py:90
  33.4 10.9 %collective-permute-start = (bf16[4,1,2,32,520]{4,3,2,1,0:T(8,128)(2,1)S(1)}, bf16[4,1,2,32,520]{4,3,2,1,0:T(8,128)(2,1)S(1)}, u32[]{:S(2)}, u32[]{:S(2)}) collective-permute-start(bf16[4,1,2,32,520]{4,3,2,1,0:T(8,128)(2,1)S(1)} %constant_dynamic-slice_fusion.1), channel_id=1, source_target_pairs={{0,4},{2,6},{4,0},{6,2},{8,12},{10,14},{12,8},{14,10},{16,20},{18,... | collective-permute-start | bytes 798728 | tf_op jit(solution)/shard_map/ppermute | solution.py:90
  37.0 8.7 %collective-permute-start.6 = (bf16[4,1,1,32,512]{4,3,2,1,0:T(8,128)(2,1)S(1)}, bf16[4,1,1,32,512]{4,3,2,1,0:T(8,128)(2,1)S(1)}, u32[]{:S(2)}, u32[]{:S(2)}) collective-permute-start(bf16[4,1,1,32,512]{4,3,2,1,0:T(8,128)(2,1)S(1)} %dynamic-slice_convert_fusion.1), channel_id=1, source_target_pairs={{0,4},{2,6},{4,0},{6,2},{8,12},{10,14},{12,8},{14,10},{16,20},{18,... | collective-permute-start | bytes 393224 | tf_op jit(solution)/shard_map/ppermute | solution.py:90
  44.4 5.4 %collective-permute-start.1 = (bf16[4,1,1,32,520]{4,3,2,1,0:T(8,128)(2,1)S(1)}, bf16[4,1,1,32,520]{4,3,2,1,0:T(8,128)(2,1)S(1)}, u32[]{:S(2)}, u32[]{:S(2)}) collective-permute-start(bf16[4,1,1,32,520]{4,3,2,1,0:T(8,128)(2,1)S(1)} %dynamic-slice_convert_fusion), channel_id=1, source_target_pairs={{0,2},{2,0},{4,6},{6,4},{8,10},{10,8},{12,14},{14,12},{16,18},{18,... | collective-permute-start | bytes 399368 | tf_op jit(solution)/shard_map/ppermute | solution.py:90
  45.8 8.6 %collective-permute-start.7 = (bf16[1,1,1,32,512]{4,3,2,1,0:T(8,128)(2,1)S(1)}, bf16[1,1,1,32,512]{4,3,2,1,0:T(8,128)(2,1)S(1)}, u32[]{:S(2)}, u32[]{:S(2)}) collective-permute-start(bf16[1,1,1,32,512]{4,3,2,1,0:T(8,128)(2,1)S(1)} %get-tuple-element.30), channel_id=1, source_target_pairs={{0,8},{2,10},{4,12},{6,14},{8,16},{10,18},{12,20},{14,22},{16,24},... | collective-permute-start | bytes 98312 | tf_op jit(solution)/shard_map/ppermute | solution.py:90
  46.1 9.1 %collective-permute-start.9 = (bf16[1,1,1,32,512]{4,3,2,1,0:T(8,128)(2,1)S(1)}, bf16[1,1,1,32,512]{4,3,2,1,0:T(8,128)(2,1)S(1)}, u32[]{:S(2)}, u32[]{:S(2)}) collective-permute-start(bf16[1,1,1,32,512]{4,3,2,1,0:T(8,128)(2,1)S(1)} %get-tuple-element.31), channel_id=1, source_target_pairs={{0,24},{2,26},{4,28},{6,30},{8,0},{10,2},{12,4},{14,6},{16,8},{18,... | collective-permute-start | bytes 98312 | tf_op jit(solution)/shard_map/ppermute | solution.py:90
  49.6 5.7 %collective-permute-start.8 = (bf16[1,1,1,32,512]{4,3,2,1,0:T(8,128)(2,1)S(1)}, bf16[1,1,1,32,512]{4,3,2,1,0:T(8,128)(2,1)S(1)}, u32[]{:S(2)}, u32[]{:S(2)}) collective-permute-start(bf16[1,1,1,32,512]{4,3,2,1,0:T(8,128)(2,1)S(1)} %get-tuple-element.32), channel_id=1, source_target_pairs={{0,16},{2,18},{4,20},{6,22},{8,24},{10,26},{12,28},{14,30},{16,0},... | collective-permute-start | bytes 98312 | tf_op jit(solution)/shard_map/ppermute | solution.py:90
  50.5 6.8 %collective-permute-start.2 = (bf16[1,1,1,32,520]{4,3,2,1,0:T(8,128)(2,1)}, bf16[1,1,1,32,520]{4,3,2,1,0:T(8,128)(2,1)S(1)}, u32[]{:S(2)}, u32[]{:S(2)}) collective-permute-start(bf16[1,1,1,32,520]{4,3,2,1,0:T(8,128)(2,1)} %get-tuple-element.27), channel_id=1, source_target_pairs={{0,8},{2,10},{4,12},{6,14},{8,16},{10,18},{12,20},{14,22},{16,24},... | collective-permute-start | bytes 99848 | tf_op jit(solution)/shard_map/ppermute | solution.py:90
  51.0 6.3 %collective-permute-start.4 = (bf16[1,1,1,32,520]{4,3,2,1,0:T(8,128)(2,1)}, bf16[1,1,1,32,520]{4,3,2,1,0:T(8,128)(2,1)S(1)}, u32[]{:S(2)}, u32[]{:S(2)}) collective-permute-start(bf16[1,1,1,32,520]{4,3,2,1,0:T(8,128)(2,1)} %get-tuple-element.28), channel_id=1, source_target_pairs={{0,24},{2,26},{4,28},{6,30},{8,0},{10,2},{12,4},{14,6},{16,8},{18,... | collective-permute-start | bytes 99848 | tf_op jit(solution)/shard_map/ppermute | solution.py:90
  54.3 5.7 %collective-permute-start.3 = (bf16[1,1,1,32,520]{4,3,2,1,0:T(8,128)(2,1)S(1)}, bf16[1,1,1,32,520]{4,3,2,1,0:T(8,128)(2,1)}, u32[]{:S(2)}, u32[]{:S(2)}) collective-permute-start(bf16[1,1,1,32,520]{4,3,2,1,0:T(8,128)(2,1)S(1)} %get-tuple-element.29), channel_id=1, source_target_pairs={{0,16},{2,18},{4,20},{6,22},{8,24},{10,26},{12,28},{14,30},{16,0},... | collective-permute-start | bytes 99848 | tf_op jit(solution)/shard_map/ppermute | solution.py:90
  70.0 4.0 %copy-start.9 = (f32[256]{0:T(256)S(1)}, f32[256]{0:T(256)}, u32[]{:S(2)}) copy-start(f32[256]{0:T(256)} %param.31) | copy-start | bytes 3076
  70.0 5.7 %copy-start.7 = (s32[32,3]{0,1:T(4,128)S(1)}, s32[32,3]{0,1:T(4,128)}, u32[]{:S(2)}) copy-start(s32[32,3]{0,1:T(4,128)} %param.40) | copy-start | bytes 1156
  70.0 5.8 %copy-start.8 = (s32[32,3]{0,1:T(4,128)S(1)}, s32[32,3]{0,1:T(4,128)}, u32[]{:S(2)}) copy-start(s32[32,3]{0,1:T(4,128)} %copy.63) | copy-start | bytes 1156
  70.0 7.1 %copy-start.3 = (bf16[32,2048]{1,0:T(8,128)(2,1)S(1)}, bf16[32,2048]{1,0:T(8,128)(2,1)}, u32[]{:S(2)}) copy-start(bf16[32,2048]{1,0:T(8,128)(2,1)} %param.21) | copy-start | bytes 393220
  70.0 7.3 %copy-start.6 = (f32[2048]{0:T(1024)S(1)}, f32[2048]{0:T(1024)}, u32[]{:S(2)}) copy-start(f32[2048]{0:T(1024)} %param.36) | copy-start | bytes 24580
  74.0 26.2 %copy-start.10 = (bf16[1,2048,704]{1,2,0:T(8,128)(2,1)S(1)}, bf16[1,2048,704]{1,2,0:T(8,128)(2,1)}, u32[]{:S(2)}) copy-start(bf16[1,2048,704]{1,2,0:T(8,128)(2,1)} %param.37) | copy-start | bytes 8650756
  75.7 1.4 collective-permute-start.10
  97.6 1.9 %collective-permute-start.11 = (bf16[16,8,2048]{2,1,0:T(8,128)(2,1)S(1)}, bf16[16,8,2048]{2,1,0:T(8,128)(2,1)S(1)}, u32[]{:S(2)}, u32[]{:S(2)}) collective-permute-start(bf16[16,8,2048]{2,1,0:T(8,128)(2,1)S(1)} %all_to_all.29), channel_id=1, source_target_pairs={{0,1},{1,0},{2,3},{3,2},{4,5},{5,4},{6,7},{7,6},{8,9},{9,8},{10,11... | collective-permute-start | bytes 1572872 | tf_op jit(solution)/shard_map/ppermute | solution.py:105
  109.6 2.0 %collective-permute-start.12 = (bf16[1,128,2048]{2,1,0:T(8,128)(2,1)S(1)}, bf16[1,128,2048]{2,1,0:T(8,128)(2,1)S(1)}, u32[]{:S(2)}, u32[]{:S(2)}) collective-permute-start(bf16[1,128,2048]{2,1,0:T(8,128)(2,1)S(1)} %slice.43), channel_id=1, source_target_pairs={{0,1},{1,0},{2,3},{3,2},{4,5},{5,4},{6,7},{7,6},{8,9},{9,8},{10,11... | collective-permute-start | bytes 1572872 | tf_op jit(solution)/shard_map/ppermute | solution.py:105
  113.6 19.3 %all-to-all-start.2 = ((bf16[16,8,2048]{2,1,0:T(8,128)(2,1)}), bf16[16,8,2048]{2,1,0:T(8,128)(2,1)S(1)}, u32[]{:S(2)}, u32[]{:S(2)}) async-start(bf16[16,8,2048]{2,1,0:T(8,128)(2,1)} %fusion.24), calls=%async_computation.2 | async-start | bytes 1048576 | tf_op jit(solution)/shard_map/all_to_all | solution.py:225
  135.6 1.7 %collective-permute-start.13 = (f32[32,2048]{1,0:T(8,128)}, f32[32,2048]{1,0:T(8,128)S(1)}, u32[]{:S(2)}, u32[]{:S(2)}) collective-permute-start(f32[32,2048]{1,0:T(8,128)} %convolution_add_fusion), channel_id=1, source_target_pairs={{0,1},{1,0},{2,3},{3,2},{4,5},{5,4},{6,7},{7,6},{8,9},{9,8},{10,11... | collective-permute-start | bytes 786440 | tf_op jit(solution)/shard_map/ppermute | solution.py:105
  (5 other events, 6.8 us)
Sparse Core Ops, SparseCore 0:
  10.7 57.9 all-gather.1

commit v2 on v1

--- a/solution.py
+++ b/solution.py
@@ -39,9 +39,7 @@
         + keep_new[:, :, None, None] * value_heads[:, :, :, None] * key_heads[:, :, None, :]
     )
     new_norm = keep_old[:, :, None] * state_norm + keep_new[:, :, None] * key_heads
-    numerator = jnp.einsum(
-        "bhvd,bhd->bhv", new_matrix, query_heads, precision=lax.Precision.HIGHEST
-    )
+    numerator = jnp.sum(new_matrix * query_heads[:, :, None, :], axis=-1)
     denominator = jnp.sum(new_norm * query_heads, axis=-1)
     cell_read = numerator / jnp.maximum(jnp.abs(denominator), jnp.exp(-new_max))[:, :, None]
     centered = cell_read - jnp.mean(cell_read, axis=-1, keepdims=True)

time: 147 us -> 144 us (0.980)
  matrix products: 19.4 us -> 16 us
  other arithmetic: 18.2 us -> 20.7 us
  local copies, waits for them, and re-layouts: 13.2 us -> 11.1 us
    reduce_sum x0 -> x1, other arithmetic: none -> 6.35 us  [memory_cell(): numerator = jnp.sum(new_matrix * query_heads[:, :, None, :], axis=-1)]
    add x1 -> x0, other arithmetic: 3.76 us -> none  [memory_cell(): keep_old[:, :, None, None] * state_matrix]
    dot_general x1 -> x0, matrix products: 3.36 us -> none  [memory_cell(): jnp.einsum('bhvd,bhd->bhv', new_matrix, query_heads, precision=lax.Precis...]
    unnamed x29 -> x27, local copies, waits for them, and re-layouts: 7.86 us -> 5.88 us
where the time goes in v2:
time: 144 us; the launch traced here: 143 us
  waiting for transfers between devices  36.3 us (25%)
  starting transfers between devices  24.3 us (17%)
  other arithmetic  20.7 us (14%)
  blocking collectives  19.9 us (14%)
  matrix products  16 us (11%)
  between operations  14.5 us (10%)
  local copies, waits for them, and re-layouts  11.1 us (8%)
    all_to_all x1, blocking collectives, body(): lax.all_to_all(outgoing, 'ep', split_axis=0, concat_axis=0, tiled=True)  19.9 us
    all_to_all x1, waiting for transfers between devices, body(): lax.all_to_all(finished, 'ep', split_axis=0, concat_axis=0, tiled=True)  14 us
    ppermute x10, waiting for transfers between devices, reduce_stage(): lax.ppermute(sent.astype(jnp.bfloat16), 'ep', shift_pairs(factors, axis,...  13.1 us
    ppermute x10, starting transfers between devices, reduce_stage(): lax.ppermute(sent.astype(jnp.bfloat16), 'ep', shift_pairs(factors, axis,...  11.8 us
    all_to_all x1, starting transfers between devices, body(): lax.all_to_all(normed, 'ep', split_axis=1, concat_axis=0, tiled=True)  8.34 us
    dot_general x1, matrix products, body(): jnp.einsum('xcf,xfd->xcd', hidden, w_expert_down, preferred_element_type=...  6.4 us
    reduce_sum x1, other arithmetic, memory_cell(): numerator = jnp.sum(new_matrix * query_heads[:, :, None, :], axis=-1)  6.35 us
    ppermute x4, waiting for transfers between devices, swap_cores(): return lax.ppermute(values_in, 'tp', [(0, 1), (1, 0)])  5.98 us
  transfers between devices with their start and end apart: 17, of which 12 were waited for; matrix products, arithmetic and copies ran while one was open for 20% of the time, Pallas kernels for 0%

profile of v2, /device:TPU:0, one launch (start us, length us, event | category | flops | bytes accessed | tf_op | source)
XLA Modules:
  0.0 143.0 jit_solution(14538455272105460633)
XLA Ops:
  9.1 1.7 %copy_bitcast_fusion = bf16[32,16,128]{2,0,1:T(8,128)(2,1)} fusion(bf16[32,2048]{1,0:T(8,128)(2,1)} %param.21, f32[2048]{0:T(1024)} %param.22, f32[32]{0:T(128)S(1)} %add_rsqrt_fusion.2), kind=kLoop, calls=%fused_computation.56 | loop fusion | flops 262144 | bytes 270464 | tf_op jit(solution)/shard_map/all_to_all | solution.py:153
  10.8 8.3 %all-to-all-start = ((bf16[32,16,128]{2,0,1:T(8,128)(2,1)}), bf16[32,16,128]{2,0,1:T(8,128)(2,1)S(1)}, u32[]{:S(2)}, u32[]{:S(2)}) async-start(bf16[32,16,128]{2,0,1:T(8,128)(2,1)} %copy_bitcast_fusion), calls=%async_computation | async-start | bytes 262144 | tf_op jit(solution)/shard_map/all_to_all | solution.py:153
  24.3 2.6 %all-to-all-done = bf16[32,16,128]{2,0,1:T(8,128)(2,1)S(1)} async-done(((bf16[32,16,128]{2,0,1:T(8,128)(2,1)}), bf16[32,16,128]{2,0,1:T(8,128)(2,1)S(1)}, u32[]{:S(2)}, u32[]{:S(2)}) %all-to-all-start) | async-done | bytes 131104 | tf_op jit(solution)/shard_map/all_to_all | solution.py:153
  30.0 2.0 %convolution_convert_fusion.2 = bf16[512,520]{0,1:T(8,128)(2,1)} fusion(bf16[512,128]{1,0:T(8,128)(2,1)S(1)} %bitcast.61, bf16[128,4]{1,0:T(8,128)(2,1)S(1)} %copy.59, bf16[128,4]{1,0:T(8,128)(2,1)S(1)} %copy.58, bf16[128,256]{1,0:T(8,128)(2,1)} %param.26, bf16[128,256]{1,0:T(8,128)(2,1)} %param.25), kind=kOutput, calls=%fused_computation.14 | convolution fusion | flops 68956160 | bytes 796672 | tf_op jit(solution)/shard_map/dot_general | solution.py:164
  33.6 2.2 %collective-permute-done.5 = bf16[4,2,1,32,512]{4,3,2,1,0:T(8,128)(2,1)} collective-permute-done((bf16[4,2,1,32,512]{4,3,2,1,0:T(8,128)(2,1)}, bf16[4,2,1,32,512]{4,3,2,1,0:T(8,128)(2,1)}, u32[]{:S(2)}, u32[]{:S(2)}) %collective-permute-start.5) | collective-permute-done | bytes 262176 | tf_op jit(solution)/shard_map/ppermute | solution.py:88
  38.0 6.3 %collective-permute-done = bf16[4,1,2,32,520]{4,3,2,1,0:T(8,128)(2,1)S(1)} collective-permute-done((bf16[4,1,2,32,520]{4,3,2,1,0:T(8,128)(2,1)S(1)}, bf16[4,1,2,32,520]{4,3,2,1,0:T(8,128)(2,1)S(1)}, u32[]{:S(2)}, u32[]{:S(2)}) %collective-permute-start) | collective-permute-done | bytes 266272 | tf_op jit(solution)/shard_map/ppermute | solution.py:88
  46.1 3.5 %collective-permute-start.9 = (bf16[1,1,1,32,512]{4,3,2,1,0:T(8,128)(2,1)S(1)}, bf16[1,1,1,32,512]{4,3,2,1,0:T(8,128)(2,1)S(1)}, u32[]{:S(2)}, u32[]{:S(2)}) collective-permute-start(bf16[1,1,1,32,512]{4,3,2,1,0:T(8,128)(2,1)S(1)} %get-tuple-element.33), channel_id=1, source_target_pairs={{0,24},{2,26},{4,28},{6,30},{8,0},{10,2},{12,4},{14,6},{16,8},{18,... | collective-permute-start | bytes 98312 | tf_op jit(solution)/shard_map/ppermute | solution.py:88
  51.0 3.3 %collective-permute-start.4 = (bf16[1,1,1,32,520]{4,3,2,1,0:T(8,128)(2,1)}, bf16[1,1,1,32,520]{4,3,2,1,0:T(8,128)(2,1)S(1)}, u32[]{:S(2)}, u32[]{:S(2)}) collective-permute-start(bf16[1,1,1,32,520]{4,3,2,1,0:T(8,128)(2,1)} %get-tuple-element.30), channel_id=1, source_target_pairs={{0,24},{2,26},{4,28},{6,30},{8,0},{10,2},{12,4},{14,6},{16,8},{18,... | collective-permute-start | bytes 99848 | tf_op jit(solution)/shard_map/ppermute | solution.py:88
  55.5 1.7 %collective-permute-done.2 = bf16[1,1,1,32,520]{4,3,2,1,0:T(8,128)(2,1)S(1)} collective-permute-done((bf16[1,1,1,32,520]{4,3,2,1,0:T(8,128)(2,1)}, bf16[1,1,1,32,520]{4,3,2,1,0:T(8,128)(2,1)S(1)}, u32[]{:S(2)}, u32[]{:S(2)}) %collective-permute-start.2) | collective-permute-done | bytes 33312 | tf_op jit(solution)/shard_map/ppermute | solution.py:88
  57.9 2.1 %collective-permute-done.3 = bf16[1,1,1,32,520]{4,3,2,1,0:T(8,128)(2,1)} collective-permute-done((bf16[1,1,1,32,520]{4,3,2,1,0:T(8,128)(2,1)S(1)}, bf16[1,1,1,32,520]{4,3,2,1,0:T(8,128)(2,1)}, u32[]{:S(2)}, u32[]{:S(2)}) %collective-permute-start.3) | collective-permute-done | bytes 33312 | tf_op jit(solution)/shard_map/ppermute | solution.py:88
  62.6 1.6 %multiply_reduce_fusion.2 = (f32[32,4]{1,0:T(8,128)S(1)}, f32[32,4,64]{2,1,0:T(4,128)}, f32[32,4,64]{2,1,0:T(4,128)S(1)}, f32[32,4,64]{2,1,0:T(4,128)S(1)}) fusion(f32[32,4,64]{2,1,0:T(4,128)S(1)} %reshape.188, f32[32,4,64]{2,1,0:T(4,128)S(1)} %reshape.187, f32[32,4]{1,0:T(8,128)S(1)} %get-tuple-element.22, f32[32,4,64]{2,1,0:T(4,128)} %param.34, ...), kind=kLoop, calls=%fused_computation.67 | loop fusion | flops 57216 | bytes 231424 | tf_op jit(solution)/shard_map/reduce_sum | solution.py:43
  64.3 6.3 %multiply_reduce_fusion = (f32[32,4,64]{2,1,0:T(4,128)S(1)}, f32[32,4,64,64]{3,2,1,0:T(8,128)}) fusion(f32[32,4,64]{2,1,0:T(4,128)S(1)} %reshape.188, f32[32,4,64]{2,1,0:T(4,128)S(1)} %get-tuple-element.35, f32[32,4,64]{2,1,0:T(4,128)S(1)} %get-tuple-element.38, f32[32,4,64,64]{3,2,1,0:T(8,128)} %param.33, f32[32,4]{1,0:T(8,128)S(1)} %subtract_exponential_fusion.1), kind=kLoop, calls=%fused_computation | loop fusion | flops 2613248 | bytes 4325888 | tf_op jit(solution)/shard_map/reduce_sum | solution.py:42
  71.3 1.6 %convolution_convert_fusion.1 = bf16[32,2048]{1,0:T(8,128)(2,1)S(1)} fusion(bf16[256,2048]{1,0:T(8,128)(2,1)} %all-gather.2.cloned.1.call-done, f32[32,256]{1,0:T(8,128)S(1)} %mul.194, bf16[32,520]{1,0:T(8,128)(2,1)S(1)} %get-tuple-element.27, f32[256]{0:T(256)S(1)} %copy-done.8), kind=kOutput, calls=%fused_computation.13 | convolution fusion | flops 33677312 | bytes 1229824 | tf_op jit(solution)/shard_map/dot_general | solution.py:190
  74.9 19.9 %all_to_all.29 = bf16[16,8,2048]{2,1,0:T(8,128)(2,1)S(1)} all-to-all(bf16[16,8,2048]{2,1,0:T(8,128)(2,1)S(1)} %fusion.12), channel_id=1, replica_groups=mesh['ep'=16,'tp'=2] {'ep'}, dimensions={0} | all-to-all | bytes 1048576 | tf_op jit(solution)/shard_map/all_to_all | solution.py:201
  94.8 1.9 %collective-permute-done.11 = bf16[16,8,2048]{2,1,0:T(8,128)(2,1)S(1)} collective-permute-done((bf16[16,8,2048]{2,1,0:T(8,128)(2,1)S(1)}, bf16[16,8,2048]{2,1,0:T(8,128)(2,1)S(1)}, u32[]{:S(2)}, u32[]{:S(2)}) %collective-permute-start.11) | collective-permute-done | bytes 524320 | tf_op jit(solution)/shard_map/ppermute | solution.py:103
  97.5 1.8 %fusion.4 = f32[256,704]{0,1:T(8,128)} fusion(bf16[1,2048,704]{1,2,0:T(8,128)(2,1)S(1)} %copy-done.9, bf16[1,128,2048]{2,1,0:T(8,128)(2,1)S(1)} %bitcast.64, bf16[1,128,2048]{2,1,0:T(8,128)(2,1)S(1)} %bitcast.62), kind=kOutput, calls=%fused_computation.6 | convolution fusion | flops 740294656 | bytes 4653056 | tf_op jit(solution)/shard_map/xcd,xdf->xcf/dot_general | solution.py:209
  99.4 6.4 %fusion.9 = bf16[1,256,2048]{2,1,0:T(8,128)(2,1)} fusion(bf16[1,704,2048]{2,1,0:T(8,128)(2,1)S(1)} %copy-done, bf16[1,2048,704]{1,2,0:T(8,128)(2,1)} %param.38, f32[256,704]{0,1:T(8,128)} %fusion.4, bf16[1,128,2048]{2,1,0:T(8,128)(2,1)} %bitcast.65, bf16[1,128,2048]{2,1,0:T(8,128)(2,1)S(1)} %bitcast.63), kind=kOutput, calls=%fused_computation.9 | convolution fusion | flops 1480097792 | bytes 8585216 | tf_op jit(solution)/shard_map/xcf,xfd->xcd/dot_general | solution.py:212
  107.0 1.8 %collective-permute-done.12 = bf16[1,128,2048]{2,1,0:T(8,128)(2,1)S(1)} collective-permute-done((bf16[1,128,2048]{2,1,0:T(8,128)(2,1)S(1)}, bf16[1,128,2048]{2,1,0:T(8,128)(2,1)S(1)}, u32[]{:S(2)}, u32[]{:S(2)}) %collective-permute-start.12) | collective-permute-done | bytes 524320 | tf_op jit(solution)/shard_map/ppermute | solution.py:103
  108.8 2.0 %fusion.24 = bf16[16,8,2048]{2,1,0:T(8,128)(2,1)} fusion(bf16[1,128,2048]{2,1,0:T(8,128)(2,1)S(1)} %collective-permute-done.12, bf16[1,256,2048]{2,1,0:T(8,128)(2,1)} %fusion.9), kind=kLoop, calls=%fused_computation.24 | loop fusion | flops 1048576 | bytes 1572864 | tf_op jit(solution)/shard_map/reshape;transpose;reshape | solution.py:222
  110.8 3.9 %all-to-all-start.2 = ((bf16[16,8,2048]{2,1,0:T(8,128)(2,1)}), bf16[16,8,2048]{2,1,0:T(8,128)(2,1)S(1)}, u32[]{:S(2)}, u32[]{:S(2)}) async-start(bf16[16,8,2048]{2,1,0:T(8,128)(2,1)} %fusion.24), calls=%async_computation.2 | async-start | bytes 1048576 | tf_op jit(solution)/shard_map/all_to_all | solution.py:223
  114.8 1.4 select_reduce_fusion
  116.2 14.0 %all-to-all-done.2 = bf16[16,8,2048]{2,1,0:T(8,128)(2,1)S(1)} async-done(((bf16[16,8,2048]{2,1,0:T(8,128)(2,1)}), bf16[16,8,2048]{2,1,0:T(8,128)(2,1)S(1)}, u32[]{:S(2)}, u32[]{:S(2)}) %all-to-all-start.2) | async-done | bytes 524320 | tf_op jit(solution)/shard_map/all_to_all | solution.py:223
  131.1 1.7 %convolution_add_fusion = f32[32,2048]{1,0:T(8,128)} fusion(f32[32,2048]{1,0:T(8,128)S(1)} %fusion.26, bf16[16,8,2048]{2,1,0:T(8,128)(2,1)S(1)} %all-to-all-done.2, f32[32,128]{1,0:T(8,128)} %select_reduce_fusion), kind=kOutput, calls=%fused_computation.12 | convolution fusion | flops 16859136 | bytes 1064960 | tf_op jit(solution)/shard_map/dot_general | solution.py:228
  134.5 1.6 %fusion.36 = bf16[32,2048]{1,0:T(8,128)(2,1)} fusion(bf16[32,2048]{1,0:T(8,128)(2,1)S(1)} %get-tuple-element.17, f32[32,2048]{1,0:T(8,128)} %convolution_add_fusion, f32[32,2048]{1,0:T(8,128)S(1)} %collective-permute-done.13), kind=kLoop, calls=%fused_computation.45 | loop fusion | flops 262144 | bytes 786432 | tf_op jit(solution)/shard_map/convert_element_type | solution.py:232
  (93 shorter events, 28.6 us)
Async XLA Ops:
  7.2 92.2 %copy-start = (bf16[1,704,2048]{2,1,0:T(8,128)(2,1)S(1)}, bf16[1,704,2048]{2,1,0:T(8,128)(2,1)}, u32[]{:S(2)}) copy-start(bf16[1,704,2048]{2,1,0:T(8,128)(2,1)} %param.39) | copy-start | bytes 8650756
  7.2 64.1 %all-gather.2.cloned.1.call-start = ((), (), s32[]{:S(2)}) async-start(), calls=%async_computation.3 | async-start | bytes 1114112 | tf_op jit(solution)/shard_map/all_gather | solution.py:132
  10.8 16.1 %all-to-all-start = ((bf16[32,16,128]{2,0,1:T(8,128)(2,1)}), bf16[32,16,128]{2,0,1:T(8,128)(2,1)S(1)}, u32[]{:S(2)}, u32[]{:S(2)}) async-start(bf16[32,16,128]{2,0,1:T(8,128)(2,1)} %copy_bitcast_fusion), calls=%async_computation | async-start | bytes 262144 | tf_op jit(solution)/shard_map/all_to_all | solution.py:153
  28.9 6.9 %collective-permute-start.5 = (bf16[4,2,1,32,512]{4,3,2,1,0:T(8,128)(2,1)}, bf16[4,2,1,32,512]{4,3,2,1,0:T(8,128)(2,1)}, u32[]{:S(2)}, u32[]{:S(2)}) collective-permute-start(bf16[4,2,1,32,512]{4,3,2,1,0:T(8,128)(2,1)} %constant_dynamic-slice_fusion), channel_id=1, source_target_pairs={{0,2},{2,0},{4,6},{6,4},{8,10},{10,8},{12,14},{14,12},{16,18},{18,... | collective-permute-start | bytes 786440 | tf_op jit(solution)/shard_map/ppermute | solution.py:88
  33.4 10.9 %collective-permute-start = (bf16[4,1,2,32,520]{4,3,2,1,0:T(8,128)(2,1)S(1)}, bf16[4,1,2,32,520]{4,3,2,1,0:T(8,128)(2,1)S(1)}, u32[]{:S(2)}, u32[]{:S(2)}) collective-permute-start(bf16[4,1,2,32,520]{4,3,2,1,0:T(8,128)(2,1)S(1)} %constant_dynamic-slice_fusion.1), channel_id=1, source_target_pairs={{0,4},{2,6},{4,0},{6,2},{8,12},{10,14},{12,8},{14,10},{16,20},{18,... | collective-permute-start | bytes 798728 | tf_op jit(solution)/shard_map/ppermute | solution.py:88
  36.9 8.7 %collective-permute-start.6 = (bf16[4,1,1,32,512]{4,3,2,1,0:T(8,128)(2,1)S(1)}, bf16[4,1,1,32,512]{4,3,2,1,0:T(8,128)(2,1)S(1)}, u32[]{:S(2)}, u32[]{:S(2)}) collective-permute-start(bf16[4,1,1,32,512]{4,3,2,1,0:T(8,128)(2,1)S(1)} %dynamic-slice_convert_fusion.1), channel_id=1, source_target_pairs={{0,4},{2,6},{4,0},{6,2},{8,12},{10,14},{12,8},{14,10},{16,20},{18,... | collective-permute-start | bytes 393224 | tf_op jit(solution)/shard_map/ppermute | solution.py:88
  44.4 5.4 %collective-permute-start.1 = (bf16[4,1,1,32,520]{4,3,2,1,0:T(8,128)(2,1)S(1)}, bf16[4,1,1,32,520]{4,3,2,1,0:T(8,128)(2,1)S(1)}, u32[]{:S(2)}, u32[]{:S(2)}) collective-permute-start(bf16[4,1,1,32,520]{4,3,2,1,0:T(8,128)(2,1)S(1)} %dynamic-slice_convert_fusion), channel_id=1, source_target_pairs={{0,2},{2,0},{4,6},{6,4},{8,10},{10,8},{12,14},{14,12},{16,18},{18,... | collective-permute-start | bytes 399368 | tf_op jit(solution)/shard_map/ppermute | solution.py:88
  45.8 8.6 %collective-permute-start.7 = (bf16[1,1,1,32,512]{4,3,2,1,0:T(8,128)(2,1)S(1)}, bf16[1,1,1,32,512]{4,3,2,1,0:T(8,128)(2,1)S(1)}, u32[]{:S(2)}, u32[]{:S(2)}) collective-permute-start(bf16[1,1,1,32,512]{4,3,2,1,0:T(8,128)(2,1)S(1)} %get-tuple-element.32), channel_id=1, source_target_pairs={{0,8},{2,10},{4,12},{6,14},{8,16},{10,18},{12,20},{14,22},{16,24},... | collective-permute-start | bytes 98312 | tf_op jit(solution)/shard_map/ppermute | solution.py:88
  46.1 9.1 %collective-permute-start.9 = (bf16[1,1,1,32,512]{4,3,2,1,0:T(8,128)(2,1)S(1)}, bf16[1,1,1,32,512]{4,3,2,1,0:T(8,128)(2,1)S(1)}, u32[]{:S(2)}, u32[]{:S(2)}) collective-permute-start(bf16[1,1,1,32,512]{4,3,2,1,0:T(8,128)(2,1)S(1)} %get-tuple-element.33), channel_id=1, source_target_pairs={{0,24},{2,26},{4,28},{6,30},{8,0},{10,2},{12,4},{14,6},{16,8},{18,... | collective-permute-start | bytes 98312 | tf_op jit(solution)/shard_map/ppermute | solution.py:88
  49.6 5.7 %collective-permute-start.8 = (bf16[1,1,1,32,512]{4,3,2,1,0:T(8,128)(2,1)S(1)}, bf16[1,1,1,32,512]{4,3,2,1,0:T(8,128)(2,1)S(1)}, u32[]{:S(2)}, u32[]{:S(2)}) collective-permute-start(bf16[1,1,1,32,512]{4,3,2,1,0:T(8,128)(2,1)S(1)} %get-tuple-element.34), channel_id=1, source_target_pairs={{0,16},{2,18},{4,20},{6,22},{8,24},{10,26},{12,28},{14,30},{16,0},... | collective-permute-start | bytes 98312 | tf_op jit(solution)/shard_map/ppermute | solution.py:88
  50.5 6.8 %collective-permute-start.2 = (bf16[1,1,1,32,520]{4,3,2,1,0:T(8,128)(2,1)}, bf16[1,1,1,32,520]{4,3,2,1,0:T(8,128)(2,1)S(1)}, u32[]{:S(2)}, u32[]{:S(2)}) collective-permute-start(bf16[1,1,1,32,520]{4,3,2,1,0:T(8,128)(2,1)} %get-tuple-element.29), channel_id=1, source_target_pairs={{0,8},{2,10},{4,12},{6,14},{8,16},{10,18},{12,20},{14,22},{16,24},... | collective-permute-start | bytes 99848 | tf_op jit(solution)/shard_map/ppermute | solution.py:88
  51.0 6.3 %collective-permute-start.4 = (bf16[1,1,1,32,520]{4,3,2,1,0:T(8,128)(2,1)}, bf16[1,1,1,32,520]{4,3,2,1,0:T(8,128)(2,1)S(1)}, u32[]{:S(2)}, u32[]{:S(2)}) collective-permute-start(bf16[1,1,1,32,520]{4,3,2,1,0:T(8,128)(2,1)} %get-tuple-element.30), channel_id=1, source_target_pairs={{0,24},{2,26},{4,28},{6,30},{8,0},{10,2},{12,4},{14,6},{16,8},{18,... | collective-permute-start | bytes 99848 | tf_op jit(solution)/shard_map/ppermute | solution.py:88
  54.3 5.7 %collective-permute-start.3 = (bf16[1,1,1,32,520]{4,3,2,1,0:T(8,128)(2,1)S(1)}, bf16[1,1,1,32,520]{4,3,2,1,0:T(8,128)(2,1)}, u32[]{:S(2)}, u32[]{:S(2)}) collective-permute-start(bf16[1,1,1,32,520]{4,3,2,1,0:T(8,128)(2,1)S(1)} %get-tuple-element.31), channel_id=1, source_target_pairs={{0,16},{2,18},{4,20},{6,22},{8,24},{10,26},{12,28},{14,30},{16,0},... | collective-permute-start | bytes 99848 | tf_op jit(solution)/shard_map/ppermute | solution.py:88
  64.2 7.1 %copy-start.8 = (f32[256]{0:T(256)S(1)}, f32[256]{0:T(256)}, u32[]{:S(2)}) copy-start(f32[256]{0:T(256)} %param.31) | copy-start | bytes 3076
  64.2 8.8 %copy-start.6 = (s32[32,3]{0,1:T(4,128)S(1)}, s32[32,3]{0,1:T(4,128)}, u32[]{:S(2)}) copy-start(s32[32,3]{0,1:T(4,128)} %param.40) | copy-start | bytes 1156
  64.2 8.7 %copy-start.7 = (s32[32,3]{0,1:T(4,128)S(1)}, s32[32,3]{0,1:T(4,128)}, u32[]{:S(2)}) copy-start(s32[32,3]{0,1:T(4,128)} %copy.63) | copy-start | bytes 1156
  64.3 10.1 %copy-start.2 = (bf16[32,2048]{1,0:T(8,128)(2,1)S(1)}, bf16[32,2048]{1,0:T(8,128)(2,1)}, u32[]{:S(2)}) copy-start(bf16[32,2048]{1,0:T(8,128)(2,1)} %param.21) | copy-start | bytes 393220
  64.3 10.2 %copy-start.5 = (f32[2048]{0:T(1024)S(1)}, f32[2048]{0:T(1024)}, u32[]{:S(2)}) copy-start(f32[2048]{0:T(1024)} %param.36) | copy-start | bytes 24580
  71.3 26.3 %copy-start.9 = (bf16[1,2048,704]{1,2,0:T(8,128)(2,1)S(1)}, bf16[1,2048,704]{1,2,0:T(8,128)(2,1)}, u32[]{:S(2)}) copy-start(bf16[1,2048,704]{1,2,0:T(8,128)(2,1)} %param.37) | copy-start | bytes 8650756
  72.9 1.4 collective-permute-start.10
  94.8 1.9 %collective-permute-start.11 = (bf16[16,8,2048]{2,1,0:T(8,128)(2,1)S(1)}, bf16[16,8,2048]{2,1,0:T(8,128)(2,1)S(1)}, u32[]{:S(2)}, u32[]{:S(2)}) collective-permute-start(bf16[16,8,2048]{2,1,0:T(8,128)(2,1)S(1)} %all_to_all.29), channel_id=1, source_target_pairs={{0,1},{1,0},{2,3},{3,2},{4,5},{5,4},{6,7},{7,6},{8,9},{9,8},{10,11... | collective-permute-start | bytes 1572872 | tf_op jit(solution)/shard_map/ppermute | solution.py:103
  106.9 2.0 %collective-permute-start.12 = (bf16[1,128,2048]{2,1,0:T(8,128)(2,1)S(1)}, bf16[1,128,2048]{2,1,0:T(8,128)(2,1)S(1)}, u32[]{:S(2)}, u32[]{:S(2)}) collective-permute-start(bf16[1,128,2048]{2,1,0:T(8,128)(2,1)S(1)} %slice.43), channel_id=1, source_target_pairs={{0,1},{1,0},{2,3},{3,2},{4,5},{5,4},{6,7},{7,6},{8,9},{9,8},{10,11... | collective-permute-start | bytes 1572872 | tf_op jit(solution)/shard_map/ppermute | solution.py:103
  110.8 19.3 %all-to-all-start.2 = ((bf16[16,8,2048]{2,1,0:T(8,128)(2,1)}), bf16[16,8,2048]{2,1,0:T(8,128)(2,1)S(1)}, u32[]{:S(2)}, u32[]{:S(2)}) async-start(bf16[16,8,2048]{2,1,0:T(8,128)(2,1)} %fusion.24), calls=%async_computation.2 | async-start | bytes 1048576 | tf_op jit(solution)/shard_map/all_to_all | solution.py:223
  132.8 1.7 %collective-permute-start.13 = (f32[32,2048]{1,0:T(8,128)}, f32[32,2048]{1,0:T(8,128)S(1)}, u32[]{:S(2)}, u32[]{:S(2)}) collective-permute-start(f32[32,2048]{1,0:T(8,128)} %convolution_add_fusion), channel_id=1, source_target_pairs={{0,1},{1,0},{2,3},{3,2},{4,5},{5,4},{6,7},{7,6},{8,9},{9,8},{10,11... | collective-permute-start | bytes 786440 | tf_op jit(solution)/shard_map/ppermute | solution.py:103
  (4 other events, 4.8 us)
Sparse Core Ops, SparseCore 0:
  10.7 57.9 all-gather.1
